TPU v7x, 32 devices: a whole 2x2x4 slice. The times are simulated.
32 devices in a mesh: sp: 16 (over z, y, core), tp: 2 (over x).
Axes of the slice: x: 2, y: 2, z: 4, core: 2. Of those that a mesh axis runs over, the one named last changes fastest.
Arguments:
- tokens_in: bfloat16 [4096, 2048], P('sp', 'tp'), may hold values from -400 to 400
- norm_gain: float32 [2048], replicated, may hold values from 0.1 to 1.9
- w_query: bfloat16 [2048, 1024], P('sp', 'tp'), may hold values from -0.125 to 0.125
- w_forget: bfloat16 [2048, 1024], P('sp', 'tp'), may hold values from -0.125 to 0.125
- w_input: bfloat16 [2048, 1024], P('sp', 'tp'), may hold values from -0.125 to 0.125
- w_rgate: bfloat16 [2048, 1024], P('sp', 'tp'), may hold values from -0.125 to 0.125
- w_pool_in: bfloat16 [2048, 1024], P('sp', 'tp'), may hold values from -0.125 to 0.125
- w_pgate: bfloat16 [2048, 1024], P('sp', 'tp'), may hold values from -0.125 to 0.125
- floor_rate: float32 [1024], P('tp'), as said below
- extra_logdecay: float32 [4096, 8], P('sp', 'tp'), as said below
- state_gain: float32 [1024], P('tp'), may hold values from 0.1 to 1.9
- pool_mix: bfloat16 [8, 128, 128], P('tp'), may hold values from -0.5 to 0.5
- pool_gain: float32 [1024], P('tp'), may hold values from 0.1 to 1.9
- out_rec: bfloat16 [1024, 2048], P('tp', 'sp'), may hold values from -0.125 to 0.125
- out_pool: bfloat16 [1024, 2048], P('tp', 'sp'), may hold values from -0.125 to 0.125
- post_gain: float32 [2048], replicated, may hold values from 0.1 to 1.9
Outputs:
- mixed_out: bfloat16 [4096, 2048], P(('sp', 'tp'))
Inputs may be any that keep to these rules, and one draw needn't show every extreme that they name: `floor_rate`: every entry is positive. `extra_logdecay`: every entry is at most zero.
All inputs are finite; a program needn't handle non-finite values.
Results may differ from a plain program's by a relative error of at most 0.015.
Values may be sent and summed in bfloat16 or wider, within the bound.
A program may use at most 64 MiB of HBM per device.

v0:
```python
import jax
import jax.numpy as jnp
from jax import lax
from jax.sharding import PartitionSpec as P

DK = 128
BLOCK = 64


eps = 1e-06
coarsest_scale_depth = lax.Precision.HIGHEST


def prefix(part, axis, combine, identity):
    place = lax.axis_index(axis)
    gathered = jax.tree.map(lambda a: lax.all_gather(a, axis), part)
    state = jax.tree.map(lambda a, e: jnp.zeros_like(a) + jnp.asarray(e, a.dtype), part, identity)

    def one(turn, state):
        return combine(
            state, jax.tree.map(lambda a: lax.dynamic_index_in_dim(a, turn, 0, False), gathered)
        )

    return lax.fori_loop(0, place, one, state)


def shifted(value, axis, steps):
    count = lax.axis_size(axis)
    initial, last = (max(0, -steps), min(count, count - steps))
    return lax.ppermute(value, axis, [(source, source + steps) for source in range(initial, last)])


def chain_merge(earlier, later):
    return (earlier[0] * later[0], later[0][..., None] * earlier[1] + later[1])


def local_blocks(qs, keys, values, logs):
    causal = jnp.arange(BLOCK)[:, None] >= jnp.arange(BLOCK)[None, :]
    heads_dev = qs.shape[1]

    def advance(carry, member):
        carried_memory_matrix, start = carry
        probe_segment, key_piece, input_piece, gc = member
        prefix_sum_vector = jnp.cumsum(gc, axis=1)
        last_index = prefix_sum_vector[:, -1]
        cross_segment_contribution = jnp.einsum(
            "abz,azy->aby",
            probe_segment * jnp.exp(prefix_sum_vector),
            carried_memory_matrix,
            precision=coarsest_scale_depth,
        )
        diff = prefix_sum_vector[:, :, None, :] - prefix_sum_vector[:, None, :, :]
        weight = jnp.where(causal[None, :, :, None], jnp.exp(jnp.minimum(diff, 0.0)), 0.0)
        scores = jnp.einsum(
            "htk,hsk,htsk->hts", probe_segment, key_piece, weight, precision=coarsest_scale_depth
        )
        final_result = cross_segment_contribution + jnp.einsum(
            "hts,hsv->htv", scores, input_piece, precision=coarsest_scale_depth
        )
        carried_memory_matrix = jnp.exp(last_index)[..., None] * carried_memory_matrix + jnp.einsum(
            "njp,njq->npq",
            key_piece * jnp.exp(last_index[:, None, :] - prefix_sum_vector),
            input_piece,
            precision=coarsest_scale_depth,
        )
        pool_reach = probe_segment * jnp.exp(start[:, None, :] + prefix_sum_vector)
        return ((carried_memory_matrix, start + last_index), (final_result, pool_reach))

    begin = (jnp.zeros((heads_dev, DK, DK), jnp.float32), jnp.zeros((heads_dev, DK), jnp.float32))
    (carried_memory_matrix, total), (final_result, pool_reach) = lax.scan(
        advance, begin, (qs, keys, values, logs)
    )
    return (carried_memory_matrix, total, final_result, pool_reach)


def per_device(
    tokens_in,
    norm_gain,
    w_query,
    w_forget,
    w_input,
    w_rgate,
    w_pool_in,
    w_pgate,
    floor_rate,
    extra_logdecay,
    state_gain,
    pool_mix,
    pool_gain,
    out_rec,
    out_pool,
    post_gain,
):
    gathered = (
        lax.all_gather(w_query, "sp", axis=0, tiled=True),
        lax.all_gather(w_forget, "sp", axis=0, tiled=True),
        lax.all_gather(w_input, "sp", axis=0, tiled=True),
        lax.all_gather(w_rgate, "sp", axis=0, tiled=True),
        lax.all_gather(w_pool_in, "sp", axis=0, tiled=True),
        lax.all_gather(w_pgate, "sp", axis=0, tiled=True),
    )
    joined = jnp.concatenate(gathered, axis=1)
    head_cols = w_query.shape[1]
    positions = tokens_in.shape[0]
    model_width = norm_gain.shape[0]
    wide = lax.all_gather(tokens_in, "tp", axis=1, tiled=True).astype(jnp.float32)
    scaled = (wide * norm_gain[None, :]).astype(jnp.bfloat16)
    totals = jnp.dot(scaled, joined, preferred_element_type=jnp.float32)
    squares = jnp.sum(wide * wide, axis=1)
    inv_rms = lax.rsqrt(squares / model_width + eps)
    proj = (totals * inv_rms[:, None]).astype(jnp.bfloat16)
    query = proj[:, 0:head_cols]
    forget = proj[:, head_cols : 2 * head_cols]
    inputs = proj[:, 2 * head_cols : 3 * head_cols]
    rgate = proj[:, 3 * head_cols : 4 * head_cols]
    pool_in = proj[:, 4 * head_cols : 5 * head_cols]
    pgate = proj[:, 5 * head_cols : 6 * head_cols]
    heads_dev = head_cols // DK
    blocks = positions // BLOCK

    def to_blocks(array):
        return array.reshape(blocks, BLOCK, heads_dev, DK).transpose(0, 2, 1, 3)

    forget32 = forget.astype(jnp.float32)
    key_gate = -jnp.expm1(-floor_rate)[None, :] * jax.nn.sigmoid(-forget32)
    log_forget = jnp.log1p(-key_gate) + jnp.repeat(extra_logdecay, DK, axis=1)
    qs = query.astype(jnp.float32) * DK ** (-0.5)
    carried_memory_matrix, total, final_result, pool_reach = local_blocks(
        to_blocks(qs),
        to_blocks(key_gate),
        to_blocks(inputs.astype(jnp.float32)),
        to_blocks(log_forget),
    )
    decays = jnp.exp(total)
    tail_rows = pool_in[positions - 16 :]
    carried = prefix(
        (decays, carried_memory_matrix),
        "sp",
        chain_merge,
        (jnp.ones_like(decays), jnp.zeros_like(carried_memory_matrix)),
    )
    incoming_state = carried[1]
    previous = shifted(tail_rows, "sp", 1).astype(jnp.float32)
    recurrent_output = final_result + jnp.einsum(
        "izaf,zfu->izau", pool_reach, incoming_state, precision=coarsest_scale_depth
    )
    grouped = recurrent_output.transpose(0, 2, 1, 3).reshape(positions, heads_dev, DK)
    normed = grouped * lax.rsqrt(jnp.mean(grouped * grouped, axis=2, keepdims=True) + eps)
    y_rec = (
        normed.reshape(positions, head_cols)
        * state_gain[None, :]
        * jax.nn.silu(rgate.astype(jnp.float32))
    ).astype(jnp.bfloat16)
    group = lax.axis_index("tp") * heads_dev + jnp.arange(head_cols) // DK
    window = jnp.power(2, 1 + group % 4).astype(jnp.int32)
    pool32 = pool_in.astype(jnp.float32)
    extended = jnp.concatenate([previous, pool32], axis=0)
    summed_rows = jnp.zeros((positions, head_cols), jnp.float32)
    for offset in range(16):
        rows_back = extended[16 - offset : 16 - offset + positions]
        summed_rows = summed_rows + jnp.where((offset < window)[None, :], rows_back, 0.0)
    place = lax.axis_index("sp") * positions + jnp.arange(positions)
    count = jnp.minimum(place[:, None] + 1, window[None, :]).astype(jnp.float32)
    mixed = (summed_rows / count - pool32).astype(jnp.bfloat16)
    mapped = jnp.einsum(
        "tgc,gcd->tgd",
        mixed.reshape(positions, heads_dev, DK),
        pool_mix,
        preferred_element_type=jnp.float32,
    ).reshape(positions, head_cols)
    y_pool = (mapped * pool_gain[None, :] * jax.nn.silu(pgate.astype(jnp.float32))).astype(
        jnp.bfloat16
    )
    out_parts = (
        lax.all_gather(out_rec, "sp", axis=1, tiled=True),
        lax.all_gather(out_pool, "sp", axis=1, tiled=True),
    )
    both = jnp.concatenate([y_rec, y_pool], axis=1)
    weight_cat = jnp.concatenate(out_parts, axis=0)
    summed = lax.psum_scatter(
        jnp.dot(both, weight_cat, preferred_element_type=jnp.float32).astype(jnp.bfloat16),
        "tp",
        scatter_dimension=0,
        tiled=True,
    ).astype(jnp.float32)
    final = (
        summed
        * lax.rsqrt(jnp.mean(summed * summed, axis=1, keepdims=True) + eps)
        * post_gain[None, :]
    )
    return final.astype(jnp.bfloat16)


def solution(mesh):
    placed = (
        P("sp", "tp"),
        P(),
        P("sp", "tp"),
        P("sp", "tp"),
        P("sp", "tp"),
        P("sp", "tp"),
        P("sp", "tp"),
        P("sp", "tp"),
        P("tp"),
        P("sp", "tp"),
        P("tp"),
        P("tp", None, None),
        P("tp"),
        P("tp", "sp"),
        P("tp", "sp"),
        P(),
    )
    return jax.shard_map(
        per_device, mesh=mesh, in_specs=placed, out_specs=P(("sp", "tp"), None), check_vma=False
    )
```

profile of v0, /device:TPU:0, one launch (start us, length us, event | category | flops | bytes accessed | tf_op | source)
XLA Modules:
  0.0 518.1 jit_solution(14276728240443677830)
XLA Ops:
  12.8 20.1 %all-gather.14.cloned.1.call-done = bf16[256,2048]{1,0:T(8,128)(2,1)} async-done(((bf16[256,1024]{1,0:T(8,128)(2,1)}), bf16[256,2048]{1,0:T(8,128)(2,1)}) %all-gather.14.cloned.1.call-update) | async-done | bytes 1048592 | tf_op jit(solution)/shard_map/all_gather | solution.py:106
  34.4 42.1 %all-gather.16.cloned.1.call-done = bf16[2048,512]{1,0:T(8,128)(2,1)} async-done(((bf16[128,512]{1,0:T(8,128)(2,1)}), bf16[2048,512]{1,0:T(8,128)(2,1)}) %all-gather.16.cloned.1.call-update) | async-done | bytes 2097168 | tf_op jit(solution)/shard_map/all_gather | solution.py:95
  76.6 3.2 constant_dynamic-update-slice_fusion.5
  79.7 39.2 %all-gather.18.cloned.1.call-done = bf16[2048,512]{1,0:T(8,128)(2,1)} async-done(((bf16[128,512]{1,0:T(8,128)(2,1)}), bf16[2048,512]{1,0:T(8,128)(2,1)}) %all-gather.18.cloned.1.call-update) | async-done | bytes 2097168 | tf_op jit(solution)/shard_map/all_gather | solution.py:96
  118.9 3.2 constant_dynamic-update-slice_fusion.4
  122.2 39.0 %all-gather.20.cloned.1.call-done = bf16[2048,512]{1,0:T(8,128)(2,1)} async-done(((bf16[128,512]{1,0:T(8,128)(2,1)}), bf16[2048,512]{1,0:T(8,128)(2,1)}) %all-gather.20.cloned.1.call-update) | async-done | bytes 2097168 | tf_op jit(solution)/shard_map/all_gather | solution.py:97
  161.2 3.1 constant_dynamic-update-slice_fusion.3
  164.3 39.1 %all-gather.22.cloned.1.call-done = bf16[2048,512]{1,0:T(8,128)(2,1)} async-done(((bf16[128,512]{1,0:T(8,128)(2,1)}), bf16[2048,512]{1,0:T(8,128)(2,1)}) %all-gather.22.cloned.1.call-update) | async-done | bytes 2097168 | tf_op jit(solution)/shard_map/all_gather | solution.py:98
  203.4 3.2 constant_dynamic-update-slice_fusion.2
  206.6 39.0 %all-gather.24.cloned.1.call-done = bf16[2048,512]{1,0:T(8,128)(2,1)} async-done(((bf16[128,512]{1,0:T(8,128)(2,1)}), bf16[2048,512]{1,0:T(8,128)(2,1)}) %all-gather.24.cloned.1.call-update) | async-done | bytes 2097168 | tf_op jit(solution)/shard_map/all_gather | solution.py:99
  245.6 3.2 constant_dynamic-update-slice_fusion.1
  248.8 39.1 %all-gather.26.cloned.1.call-done = bf16[2048,512]{1,0:T(8,128)(2,1)} async-done(((bf16[128,512]{1,0:T(8,128)(2,1)}), bf16[2048,512]{1,0:T(8,128)(2,1)}) %all-gather.26.cloned.1.call-update) | async-done | bytes 2097168 | tf_op jit(solution)/shard_map/all_gather | solution.py:100
  288.0 3.1 constant_dynamic-update-slice_fusion
  291.1 8.0 %fusion.29 = bf16[256,3072]{1,0:T(8,128)(2,1)S(1)} fusion(bf16[2048,3072]{1,0:T(8,128)(2,1)} %constant_dynamic-update-slice_fusion, f32[256]{0:T(256)S(1)} %add_rsqrt_fusion.1, bf16[256,2048]{1,0:T(8,128)(2,1)S(1)} %copy-done.3, f32[2048]{0:T(1024)S(1)} %copy-done.10), kind=kOutput, calls=%fused_computation.44 | convolution fusion | flops 3224371200 | bytes 15213568 | tf_op jit(solution)/shard_map/dot_general | solution.py:108
  301.9 48.2 %while.30 = (s32[]{:T(128)}, f32[4,128,128]{2,1,0:T(8,128)S(1)}, f32[4,128]{1,0:T(4,128)S(1)}, f32[4,4,64,128]{3,2,0,1:T(8,128)}, f32[4,4,64,128]{3,2,0,1:T(8,12...) while((s32[]{:T(128)}, f32[4,128,128]{2,1,0:T(8,128)S(1)}, ...), condition=%wide.region_3.4_spmd.clone, body=%wide.region_1.3_spmd.clone.sunk | while | flops 140923904 | bytes 20806288 | solution.py:70
  302.3 1.7 exponential_select_fusion.2
  304.0 7.3 %fusion.136 = f32[4,64,64]{1,2,0:T(8,128)S(1)} fusion(f32[4,64,64,128]{3,2,1,0:T(8,128)S(1)} %exponential_select_fusion.2, f32[4,128,64]{1,2,0:T(8,128)S(1)} %dynamic-slice_bitcast_fusion.9, f32[4,128,64]{1,2,0:T(8,128)S(1)} %get-tuple-element.298), kind=kLoop, calls=%fused_computation.4.clone.1 | loop fusion | flops 6275072 | bytes 8716288 | tf_op jit(solution)/shard_map/while/body/eval_jaxpr/htk,hsk,htsk->hts/dot_general | solution.py:54
  314.3 1.7 exponential_select_fusion.2
  316.0 7.3 %fusion.136 = f32[4,64,64]{1,2,0:T(8,128)S(1)} fusion(f32[4,64,64,128]{3,2,1,0:T(8,128)S(1)} %exponential_select_fusion.2, f32[4,128,64]{1,2,0:T(8,128)S(1)} %dynamic-slice_bitcast_fusion.9, f32[4,128,64]{1,2,0:T(8,128)S(1)} %get-tuple-element.298), kind=kLoop, calls=%fused_computation.4.clone.1 | loop fusion | flops 6275072 | bytes 8716288 | tf_op jit(solution)/shard_map/while/body/eval_jaxpr/htk,hsk,htsk->hts/dot_general | solution.py:54
  326.3 1.7 exponential_select_fusion.2
  328.0 7.3 %fusion.136 = f32[4,64,64]{1,2,0:T(8,128)S(1)} fusion(f32[4,64,64,128]{3,2,1,0:T(8,128)S(1)} %exponential_select_fusion.2, f32[4,128,64]{1,2,0:T(8,128)S(1)} %dynamic-slice_bitcast_fusion.9, f32[4,128,64]{1,2,0:T(8,128)S(1)} %get-tuple-element.298), kind=kLoop, calls=%fused_computation.4.clone.1 | loop fusion | flops 6275072 | bytes 8716288 | tf_op jit(solution)/shard_map/while/body/eval_jaxpr/htk,hsk,htsk->hts/dot_general | solution.py:54
  338.3 1.7 exponential_select_fusion.2
  340.0 7.3 %fusion.136 = f32[4,64,64]{1,2,0:T(8,128)S(1)} fusion(f32[4,64,64,128]{3,2,1,0:T(8,128)S(1)} %exponential_select_fusion.2, f32[4,128,64]{1,2,0:T(8,128)S(1)} %dynamic-slice_bitcast_fusion.9, f32[4,128,64]{1,2,0:T(8,128)S(1)} %get-tuple-element.298), kind=kLoop, calls=%fused_computation.4.clone.1 | loop fusion | flops 6275072 | bytes 8716288 | tf_op jit(solution)/shard_map/while/body/eval_jaxpr/htk,hsk,htsk->hts/dot_general | solution.py:54
  353.2 2.1 collective-permute-start
  355.4 19.7 %all-gather.2 = f32[16,4,128]{2,1,0:T(4,128)S(1)} all-gather(f32[1,4,128]{2,1,0:T(4,128)S(1)} %exponential_bitcast_fusion), channel_id=2, replica_groups=mesh['sp'=16,'tp'=2] {'sp'}, dimensions={0}, use_global_device_ids=true | all-gather | bytes 34816 | tf_op jit(solution)/shard_map/all_gather | solution.py:16
  375.1 1.7 fusion.103
  377.0 23.2 %all-gather.32.cloned.1.call-done = f32[64,128,128]{2,1,0:T(8,128)} async-done(((f32[4,128,128]{2,1,0:T(8,128)}), f32[64,128,128]{2,1,0:T(8,128)}) %all-gather.32.cloned.1.call-update) | async-done | bytes 4194320 | tf_op jit(solution)/shard_map/all_gather | solution.py:16
  403.2 38.8 %all-gather.28.cloned.1.call-done = bf16[512,2048]{1,0:T(8,128)(2,1)} async-done(((bf16[512,128]{1,0:T(8,128)(2,1)}), bf16[512,2048]{1,0:T(8,128)(2,1)}) %all-gather.28.cloned.1.call-update) | async-done | bytes 2097168 | tf_op jit(solution)/shard_map/all_gather | solution.py:175
  442.0 42.2 %all-gather.30.cloned.1.call-done = bf16[512,2048]{1,0:T(8,128)(2,1)} async-done(((bf16[512,128]{1,0:T(8,128)(2,1)}), bf16[512,2048]{1,0:T(8,128)(2,1)}) %all-gather.30.cloned.1.call-update) | async-done | bytes 2097168 | tf_op jit(solution)/shard_map/all_gather | solution.py:176
  484.1 4.5 fusion.30
  488.6 19.6 %reduce-scatter.2.cloned.1.call-done = bf16[128,2048]{1,0:T(8,128)(2,1)} async-done(((bf16[256,2048]{1,0:T(8,128)(2,1)}), bf16[128,2048]{1,0:T(8,128)(2,1)}) %reduce-scatter.2.cloned.1.call-update) | async-done | bytes 524304 | tf_op jit(solution)/shard_map/reduce_scatter | solution.py:180
  509.5 2.0 fusion.39
  (126 shorter events, 29.7 us)
Async XLA Ops:
  6.5 368.5 %copy-start = (bf16[4,128,128]{2,1,0:T(8,128)(2,1)S(1)}, bf16[4,128,128]{2,1,0:T(8,128)(2,1)}, u32[]{:S(2)}) copy-start(bf16[4,128,128]{2,1,0:T(8,128)(2,1)} %param.31) | copy-start | bytes 393220
  6.5 26.4 %all-gather.14.cloned.1.call-start = ((), (), s32[]{:S(2)}) async-start(), calls=%async_computation.1 | async-start | bytes 1572864 | tf_op jit(solution)/shard_map/all_gather | solution.py:106
  7.3 69.3 %all-gather.16.cloned.1.call-start = ((), (), s32[]{:S(2)}) async-start(), calls=%async_computation.2 | async-start | bytes 2228224 | tf_op jit(solution)/shard_map/all_gather | solution.py:95
  8.0 110.9 %all-gather.18.cloned.1.call-start = ((), (), s32[]{:S(2)}) async-start(), calls=%async_computation.3 | async-start | bytes 2228224 | tf_op jit(solution)/shard_map/all_gather | solution.py:96
  8.7 152.4 %all-gather.20.cloned.1.call-start = ((), (), s32[]{:S(2)}) async-start(), calls=%async_computation.4 | async-start | bytes 2228224 | tf_op jit(solution)/shard_map/all_gather | solution.py:97
  9.3 194.1 %all-gather.22.cloned.1.call-start = ((), (), s32[]{:S(2)}) async-start(), calls=%async_computation.5 | async-start | bytes 2228224 | tf_op jit(solution)/shard_map/all_gather | solution.py:98
  9.9 235.7 %all-gather.24.cloned.1.call-start = ((), (), s32[]{:S(2)}) async-start(), calls=%async_computation.6 | async-start | bytes 2228224 | tf_op jit(solution)/shard_map/all_gather | solution.py:99
  10.5 277.5 %all-gather.26.cloned.1.call-start = ((), (), s32[]{:S(2)}) async-start(), calls=%async_computation.7 | async-start | bytes 2228224 | tf_op jit(solution)/shard_map/all_gather | solution.py:100
  11.2 389.0 %all-gather.32.cloned.1.call-start = ((), (), s32[]{:S(2)}) async-start(), calls=%async_computation.11 | async-start | bytes 4456448 | tf_op jit(solution)/shard_map/all_gather | solution.py:16
  206.6 84.5 %copy-start.3 = (bf16[256,2048]{1,0:T(8,128)(2,1)S(1)}, bf16[256,2048]{1,0:T(8,128)(2,1)}, u32[]{:S(2)}) copy-start(bf16[256,2048]{1,0:T(8,128)(2,1)} %all-gather.14.cloned.1.call-done) | copy-start | bytes 3145732
  206.6 84.5 %copy-start.10 = (f32[2048]{0:T(1024)S(1)}, f32[2048]{0:T(1024)}, u32[]{:S(2)}) copy-start(f32[2048]{0:T(1024)} %param.21) | copy-start | bytes 24580
  299.1 1.7 copy-start.2
  301.9 73.2 %copy-start.4 = (f32[256,512]{1,0:T(8,128)S(1)}, f32[256,512]{1,0:T(8,128)}, u32[]{:S(2)}) copy-start(f32[256,512]{1,0:T(8,128)} %get-tuple-element.180) | copy-start | bytes 1572868
  350.1 0.7 copy-start.1
  350.9 91.1 %all-gather.28.cloned.1.call-start = ((), (), s32[]{:S(2)}) async-start(), calls=%async_computation.8 | async-start | bytes 2228224 | tf_op jit(solution)/shard_map/all_gather | solution.py:175
  351.6 132.5 %all-gather.30.cloned.1.call-start = ((), (), s32[]{:S(2)}) async-start(), calls=%async_computation.9 | async-start | bytes 2228224 | tf_op jit(solution)/shard_map/all_gather | solution.py:176
  352.2 156.1 %reduce-scatter.2.cloned.1.call-start = ((), (), s32[]{:S(2)}) async-start(), calls=%async_computation.10 | async-start | bytes 1572864 | tf_op jit(solution)/shard_map/reduce_scatter | solution.py:180
  353.2 21.8 %collective-permute-start = (bf16[16,512]{1,0:T(8,128)(2,1)S(1)}, bf16[16,512]{1,0:T(8,128)(2,1)S(1)}, u32[]{:S(2)}, u32[]{:S(2)}) collective-permute-start(bf16[16,512]{1,0:T(8,128)(2,1)S(1)} %slice.99), channel_id=1, source_target_pairs={{0,2},{2,4},{4,6},{6,8},{8,10},{10,12},{12,14},{14,16},{16,18},{18... | collective-permute-start | bytes 49160 | tf_op jit(solution)/shard_map/ppermute | solution.py:30
  376.8 23.4 %copy-start.5 = (f32[4,4,64,128]{3,2,0,1:T(8,128)S(1)}, f32[4,4,64,128]{3,2,0,1:T(8,128)}, u32[]{:S(2)}) copy-start(f32[4,4,64,128]{3,2,0,1:T(8,128)} %get-tuple-element.104) | copy-start | bytes 1572868
  376.8 23.4 %copy-start.6 = (f32[4,4,64,128]{3,2,0,1:T(8,128)S(1)}, f32[4,4,64,128]{3,2,0,1:T(8,128)}, u32[]{:S(2)}) copy-start(f32[4,4,64,128]{3,2,0,1:T(8,128)} %get-tuple-element.108) | copy-start | bytes 1572868
  377.0 24.8 %copy-start.8 = (f32[512]{0:T(512)S(1)}, f32[512]{0:T(512)}, u32[]{:S(2)}) copy-start(f32[512]{0:T(512)} %param.30) | copy-start | bytes 6148
  377.0 24.8 %copy-start.9 = (f32[512]{0:T(512)S(1)}, f32[512]{0:T(512)}, u32[]{:S(2)}) copy-start(f32[512]{0:T(512)} %param.32) | copy-start | bytes 6148
  484.1 25.4 %copy-start.7 = (f32[2048]{0:T(1024)S(1)}, f32[2048]{0:T(1024)}, u32[]{:S(2)}) copy-start(f32[2048]{0:T(1024)} %param.35) | copy-start | bytes 24580
Sparse Core Ops, SparseCore 0:
  8.9 23.9 all-gather.13
  35.1 41.4 all-gather.15
  78.7 40.1 all-gather.17
  121.0 40.1 all-gather.19
  163.2 40.1 all-gather.21
  205.4 40.1 all-gather.23
  247.8 40.1 all-gather.25
  351.0 49.1 all-gather.31
  402.4 39.5 all-gather.27
  444.0 40.1 all-gather.29
  488.8 19.4 reduce-scatter.1
where the time goes:
time: 519 us; the launch traced here: 518 us
  waiting for transfers between devices  387 us (75%)
  other arithmetic  47.9 us (9%)
  local copies, waits for them, and re-layouts  23.9 us (5%)
  matrix products  23.2 us (4%)
  blocking collectives  19.7 us (4%)
  between operations  13.6 us (3%)
    all_gather x1, waiting for transfers between devices, per_device(): lax.all_gather(out_pool, 'sp', axis=1, tiled=True)  42.2 us
    all_gather x1, waiting for transfers between devices, per_device(): lax.all_gather(w_query, 'sp', axis=0, tiled=True)  42.1 us
    all_gather x1, waiting for transfers between devices, per_device(): lax.all_gather(w_forget, 'sp', axis=0, tiled=True)  39.2 us
    all_gather x1, waiting for transfers between devices, per_device(): lax.all_gather(w_pgate, 'sp', axis=0, tiled=True)  39.1 us
    all_gather x1, waiting for transfers between devices, per_device(): lax.all_gather(w_rgate, 'sp', axis=0, tiled=True)  39.1 us
    all_gather x1, waiting for transfers between devices, per_device(): lax.all_gather(w_pool_in, 'sp', axis=0, tiled=True)  39 us
    all_gather x1, waiting for transfers between devices, per_device(): lax.all_gather(w_input, 'sp', axis=0, tiled=True)  39 us
    all_gather x1, waiting for transfers between devices, per_device(): lax.all_gather(out_rec, 'sp', axis=1, tiled=True)  38.8 us
  transfers between devices with their start and end apart: 12, of which 11 were waited for; matrix products, arithmetic and copies ran while one was open for 5% of the time, Pallas kernels for 0%

commit v1 on v0

--- a/solution.py
+++ b/solution.py
@@ -1,6 +1,8 @@
 import jax
 import jax.numpy as jnp
 from jax import lax
+from jax.experimental import pallas as pl
+from jax.experimental.pallas import tpu as pltpu
 from jax.sharding import PartitionSpec as P
 
 DK = 128
@@ -28,6 +30,246 @@
     count = lax.axis_size(axis)
     initial, last = (max(0, -steps), min(count, count - steps))
     return lax.ppermute(value, axis, [(source, source + steps) for source in range(initial, last)])
+
+
+PIECES = 2
+
+
+def ring_place(chip, chips):
+    odd = chip % 2
+    return (1 - odd) * (chip // 2) + odd * (chips - 1 - chip // 2)
+
+
+def ring_chip(place, chips):
+    back = place // (chips // 2)
+    return (1 - back) * (2 * place) + back * (2 * (chips - 1 - place) + 1)
+
+
+def project_kernel(
+    n,
+    n_tp,
+    tok_ref,
+    gain_ref,
+    w_ref,
+    proj_ref,
+    wide,
+    scaled,
+    weights,
+    acc,
+    tok_send,
+    tok_recv,
+    own_sem,
+    ring_send,
+    ring_recv,
+    core_send,
+    core_recv,
+):
+    chips = n // 2
+    steps = chips // 2
+    me = lax.axis_index("sp")
+    tp = lax.axis_index("tp")
+    core = me % 2
+    place = ring_place(me // 2, chips)
+
+    def chip_at(offset):
+        return ring_chip((place + offset + chips) % chips, chips)
+
+    following = 2 * chip_at(1) + core
+    preceding = 2 * chip_at(-1) + core
+    partner = 2 * (me // 2) + 1 - core
+    rows = w_ref.shape[0]
+    piece = rows // PIECES
+    features = tok_ref.shape[1]
+
+    barrier = pltpu.get_barrier_semaphore()
+    for peer in (following, preceding, partner):
+        pl.semaphore_signal(barrier, inc=1, device_id={"sp": peer})
+    for turn in range(1, n_tp):
+        pl.semaphore_signal(barrier, inc=1, device_id={"tp": (tp + turn) % n_tp})
+    pl.semaphore_wait(barrier, 3 + n_tp - 1)
+
+    def rows_of(chip, which, q):
+        start = (2 * chip + which) * rows + q * piece
+        return pl.ds(pl.multiple_of(start, 16), piece)
+
+    sends = []
+
+    def to_core(offset, q, source):
+        slot = offset + steps - 1
+        copy = pltpu.make_async_remote_copy(
+            src_ref=source,
+            dst_ref=weights.at[rows_of(chip_at(offset), core, q)],
+            send_sem=core_send.at[slot, q],
+            recv_sem=core_recv.at[slot, q],
+            device_id={"sp": partner},
+        )
+        copy.start()
+        sends.append(copy)
+
+    def from_core(offset, q):
+        slot = offset + steps - 1
+        dst = weights.at[rows_of(chip_at(offset), 1 - core, q)]
+        pltpu.make_async_remote_copy(
+            src_ref=dst,
+            dst_ref=dst,
+            send_sem=core_send.at[slot, q],
+            recv_sem=core_recv.at[slot, q],
+            device_id={"sp": partner},
+        ).wait_recv()
+
+    def pieces_of(direction, step):
+        if step < steps - 1:
+            return range(PIECES)
+        half = PIECES // 2
+        return range(half) if direction == 0 else range(half, PIECES)
+
+    def ring_copy(direction, step, q, source):
+        offset = -step if direction == 0 else step
+        dst = weights.at[rows_of(chip_at(offset), core, q)]
+        return pltpu.make_async_remote_copy(
+            src_ref=dst if source is None else source,
+            dst_ref=dst,
+            send_sem=ring_send.at[direction, step, q],
+            recv_sem=ring_recv.at[direction, step, q],
+            device_id={"sp": following if direction == 0 else preceding},
+        )
+
+    def ring_arrival(direction, step, q):
+        offset = -(step + 1) if direction == 0 else step + 1
+        dst = weights.at[rows_of(chip_at(offset), core, q)]
+        pltpu.make_async_remote_copy(
+            src_ref=dst,
+            dst_ref=dst,
+            send_sem=ring_send.at[direction, step, q],
+            recv_sem=ring_recv.at[direction, step, q],
+            device_id={"sp": following if direction == 0 else preceding},
+        ).wait_recv()
+
+    for q in range(PIECES):
+        mine = w_ref.at[pl.ds(q * piece, piece)]
+        for direction in range(2):
+            if q in pieces_of(direction, 0):
+                copy = ring_copy(direction, 0, q, mine)
+                copy.start()
+                sends.append(copy)
+        to_core(0, q, mine)
+    tokens_at = pl.ds(pl.multiple_of(tp * features, 128), features)
+    for turn in range(1, n_tp):
+        copy = pltpu.make_async_remote_copy(
+            src_ref=tok_ref,
+            dst_ref=wide.at[:, tokens_at],
+            send_sem=tok_send.at[turn - 1],
+            recv_sem=tok_recv.at[turn - 1],
+            device_id={"tp": (tp + turn) % n_tp},
+        )
+        copy.start()
+        sends.append(copy)
+    own = pltpu.make_async_copy(
+        w_ref, weights.at[pl.ds(pl.multiple_of(me * rows, 16), rows)], own_sem
+    )
+    own.start()
+    acc[...] = jnp.zeros_like(acc)
+    wide[:, tokens_at] = tok_ref[...]
+    for turn in range(1, n_tp):
+        theirs = pl.ds(
+            pl.multiple_of((tp - turn + n_tp) % n_tp * features, 128), features
+        )
+        pltpu.make_async_remote_copy(
+            src_ref=tok_ref,
+            dst_ref=wide.at[:, theirs],
+            send_sem=tok_send.at[turn - 1],
+            recv_sem=tok_recv.at[turn - 1],
+            device_id={"tp": (tp + turn) % n_tp},
+        ).wait_recv()
+    scaled[...] = (wide[...].astype(jnp.float32) * gain_ref[...]).astype(jnp.bfloat16)
+
+    cols = weights.shape[1]
+    tile = cols // 6
+
+    by_chip = (2 * rows) % 128 == 0
+
+    def multiply(offset):
+        if not by_chip:
+            return
+        multiply_rows(pl.ds(pl.multiple_of(chip_at(offset) * 2 * rows, 2 * rows), 2 * rows))
+
+    def multiply_rows(depth):
+        def one(i, _):
+            at = pl.ds(pl.multiple_of(i * tile, 128), tile)
+            acc[:, at] += jnp.dot(
+                scaled[:, depth], weights[depth, at], preferred_element_type=jnp.float32
+            )
+            return 0
+
+        lax.fori_loop(0, 6, one, 0)
+
+    own.wait()
+    for step in range(steps):
+        for q in range(PIECES):
+            for direction in range(2):
+                if q not in pieces_of(direction, step):
+                    continue
+                offset = -(step + 1) if direction == 0 else step + 1
+                ring_arrival(direction, step, q)
+                if step + 1 < steps and q in pieces_of(direction, step + 1):
+                    copy = ring_copy(direction, step + 1, q, None)
+                    copy.start()
+                    sends.append(copy)
+                last = offset if abs(offset) < steps else steps
+                dst = weights.at[rows_of(chip_at(last), core, q)]
+                to_core(last, q, dst)
+        for offset in [0] if step == 0 else [-step, step]:
+            for q in range(PIECES):
+                from_core(offset, q)
+            multiply(offset)
+    for q in range(PIECES):
+        from_core(steps, q)
+    multiply(steps)
+    if not by_chip:
+        multiply_rows(slice(None))
+    values = wide[...].astype(jnp.float32)
+    squares = jnp.sum(values * values, axis=1, keepdims=True)
+    inv_rms = lax.rsqrt(squares / wide.shape[1] + eps)
+    proj_ref[...] = (acc[...] * inv_rms).astype(jnp.bfloat16)
+    for copy in sends:
+        copy.wait_send()
+
+
+def project(tokens, gain, shard):
+    import functools
+
+    n = lax.axis_size("sp")
+    n_tp = lax.axis_size("tp")
+    positions, features = tokens.shape
+    rows, cols = shard.shape
+    width = n * rows
+    steps = n // 4
+    dma = pltpu.SemaphoreType.DMA
+    return pl.pallas_call(
+        functools.partial(project_kernel, n, n_tp),
+        out_shape=jax.ShapeDtypeStruct((positions, cols), jnp.bfloat16),
+        in_specs=[pl.BlockSpec(memory_space=pltpu.VMEM)] * 3,
+        out_specs=pl.BlockSpec(memory_space=pltpu.VMEM),
+        scratch_shapes=[
+            pltpu.VMEM((positions, width), jnp.bfloat16),
+            pltpu.VMEM((positions, width), jnp.bfloat16),
+            pltpu.VMEM((width, cols), jnp.bfloat16),
+            pltpu.VMEM((positions, cols), jnp.float32),
+            dma((n_tp,)),
+            dma((n_tp,)),
+            dma,
+            dma((2, steps, PIECES)),
+            dma((2, steps, PIECES)),
+            dma((2 * steps, PIECES)),
+            dma((2 * steps, PIECES)),
+        ],
+        compiler_params=pltpu.CompilerParams(
+            collective_id=0, has_side_effects=True, vmem_limit_bytes=56 * 1024 * 1024
+        ),
+        cost_estimate=pl.CostEstimate(
+            flops=2 * positions * width * cols, bytes_accessed=4 * rows * cols, transcendentals=0
+        ),
+    )(tokens, gain[None, :], shard)
 
 
 def chain_merge(earlier, later):
@@ -91,24 +333,12 @@
     out_pool,
     post_gain,
 ):
-    gathered = (
-        lax.all_gather(w_query, "sp", axis=0, tiled=True),
-        lax.all_gather(w_forget, "sp", axis=0, tiled=True),
-        lax.all_gather(w_input, "sp", axis=0, tiled=True),
-        lax.all_gather(w_rgate, "sp", axis=0, tiled=True),
-        lax.all_gather(w_pool_in, "sp", axis=0, tiled=True),
-        lax.all_gather(w_pgate, "sp", axis=0, tiled=True),
-    )
-    joined = jnp.concatenate(gathered, axis=1)
+    shard = jnp.concatenate(
+        [w_query, w_forget, w_input, w_rgate, w_pool_in, w_pgate], axis=1
+    )
     head_cols = w_query.shape[1]
     positions = tokens_in.shape[0]
-    model_width = norm_gain.shape[0]
-    wide = lax.all_gather(tokens_in, "tp", axis=1, tiled=True).astype(jnp.float32)
-    scaled = (wide * norm_gain[None, :]).astype(jnp.bfloat16)
-    totals = jnp.dot(scaled, joined, preferred_element_type=jnp.float32)
-    squares = jnp.sum(wide * wide, axis=1)
-    inv_rms = lax.rsqrt(squares / model_width + eps)
-    proj = (totals * inv_rms[:, None]).astype(jnp.bfloat16)
+    proj = project(tokens_in, norm_gain, shard)
     query = proj[:, 0:head_cols]
     forget = proj[:, head_cols : 2 * head_cols]
     inputs = proj[:, 2 * head_cols : 3 * head_cols]

time: 519 us -> 311 us (0.60)
  waiting for transfers between devices: 387 us -> 125 us
  Pallas kernels: 0 us -> 73.3 us
  local copies, waits for them, and re-layouts: 23.9 us -> 11.2 us
  matrix products: 23.2 us -> 15.2 us
    all_gather x7 -> x0, waiting for transfers between devices: 258 us -> none  [the longest x1 42.1 us: per_device(): lax.all_gather(w_query, 'sp', axis=0, tiled=True)]
    pallas_call x0 -> x1, Pallas kernels: none -> 73.3 us  [project(): pl.pallas_call(functools.partial(project_kernel, n, n_tp), out_shape=jax....]
    unnamed x29 -> x25, local copies, waits for them, and re-layouts: 17.6 us -> 7.03 us
    dot_general x1 -> x0, matrix products: 7.99 us -> none  [per_device(): totals = jnp.dot(scaled, joined, preferred_element_type=jnp.float32)]
  transfers between devices with their start and end apart: 12 -> 5, of which waited for: 11 -> 4; matrix products, arithmetic and copies ran while one was open for 5% -> 2% of each run, Pallas kernels for 0% -> 0%
where the time goes in v1:
time: 311 us; the launch traced here: 310 us
  waiting for transfers between devices  125 us (40%)
  Pallas kernels  73.3 us (24%)
  other arithmetic  48.3 us (16%)
  blocking collectives  21.7 us (7%)
  matrix products  15.2 us (5%)
  between operations  13.4 us (4%)
  local copies, waits for them, and re-layouts  11.2 us (4%)
    pallas_call x1, Pallas kernels, project(): pl.pallas_call(functools.partial(project_kernel, n, n_tp), out_shape=jax....  73.3 us
    all_gather x1, waiting for transfers between devices, per_device(): lax.all_gather(out_pool, 'sp', axis=1, tiled=True)  42.3 us
    all_gather x1, waiting for transfers between devices, per_device(): lax.all_gather(out_rec, 'sp', axis=1, tiled=True)  38.7 us
    dot_general x4, other arithmetic, advance(): jnp.einsum('htk,hsk,htsk->hts', probe_segment, key_piece, weight, precisi...  29.3 us
    all_gather x1, waiting for transfers between devices, prefix(): gathered = jax.tree.map(lambda a: lax.all_gather(a, axis), part)  23.6 us
    all_gather x1, blocking collectives, prefix(): gathered = jax.tree.map(lambda a: lax.all_gather(a, axis), part)  21.7 us
    reduce_scatter x1, waiting for transfers between devices, per_device(): lax.psum_scatter(jnp.dot(both, weight_cat, preferred_element_type=jnp.flo...  19.6 us
    unnamed x25, local copies, waits for them, and re-layouts  7.03 us
  transfers between devices with their start and end apart: 5, of which 4 were waited for; matrix products, arithmetic and copies ran while one was open for 2% of the time, Pallas kernels for 0%

profile of v1, /device:TPU:0, one launch (start us, length us, event | category | flops | bytes accessed | tf_op | source)
XLA Modules:
  0.0 310.1 jit_solution(6964322864808657732)
XLA Ops:
  6.5 1.0 constant_dynamic-update-slice_fusion.5
  9.0 0.9 constant_dynamic-update-slice_fusion.4
  9.9 0.9 constant_dynamic-update-slice_fusion.3
  10.9 0.9 constant_dynamic-update-slice_fusion.2
  12.7 0.9 constant_dynamic-update-slice_fusion.w_ref
  14.5 73.3 %shard_map.154 = bf16[256,3072]{1,0:T(8,128)(2,1)} custom-call(bf16[256,1024]{1,0:T(8,128)(2,1)} %tok_ref.1, f32[1,2048]{1,0:T(1,128)} %bitcast.141, bf16[128,3072]{1,0:T(8,128)(2,1)} %copy-done.5), custom_call_target="tpu_custom_call" | custom-call | flops 3221225472 | bytes 1572864 | tf_op jit(solution)/shard_map/pallas_call | solution.py:248
  87.8 2.0 slice_convert_fusion.1
  90.1 1.4 divide_multiply_fusion
  92.6 48.3 %while.30 = (s32[]{:T(128)}, f32[4,128,128]{2,1,0:T(8,128)S(1)}, f32[4,128]{1,0:T(4,128)S(1)}, f32[4,4,64,128]{3,2,0,1:T(8,128)}, f32[4,4,64,128]{3,2,0,1:T(8,12...) while((s32[]{:T(128)}, f32[4,128,128]{2,1,0:T(8,128)S(1)}, ...), condition=%wide.region_2.3_spmd.clone, body=%wide.region_0.2_spmd.clone.sunk | while | flops 140923904 | bytes 20806288 | solution.py:312
  92.9 1.7 exponential_select_fusion.2
  94.7 7.3 %fusion.130 = f32[4,64,64]{1,2,0:T(8,128)S(1)} fusion(f32[4,64,64,128]{3,2,1,0:T(8,128)S(1)} %exponential_select_fusion.2, f32[4,128,64]{1,2,0:T(8,128)S(1)} %dynamic-slice_bitcast_fusion.9, f32[4,128,64]{1,2,0:T(8,128)S(1)} %get-tuple-element.298), kind=kLoop, calls=%fused_computation.4.clone.1 | loop fusion | flops 6275072 | bytes 8716288 | tf_op jit(solution)/shard_map/while/body/eval_jaxpr/htk,hsk,htsk->hts/dot_general | solution.py:296
  102.4 1.0 fusion.132
  105.0 1.7 exponential_select_fusion.2
  106.7 7.3 %fusion.130 = f32[4,64,64]{1,2,0:T(8,128)S(1)} fusion(f32[4,64,64,128]{3,2,1,0:T(8,128)S(1)} %exponential_select_fusion.2, f32[4,128,64]{1,2,0:T(8,128)S(1)} %dynamic-slice_bitcast_fusion.9, f32[4,128,64]{1,2,0:T(8,128)S(1)} %get-tuple-element.298), kind=kLoop, calls=%fused_computation.4.clone.1 | loop fusion | flops 6275072 | bytes 8716288 | tf_op jit(solution)/shard_map/while/body/eval_jaxpr/htk,hsk,htsk->hts/dot_general | solution.py:296
  114.4 1.0 fusion.132
  117.0 1.7 exponential_select_fusion.2
  118.7 7.3 %fusion.130 = f32[4,64,64]{1,2,0:T(8,128)S(1)} fusion(f32[4,64,64,128]{3,2,1,0:T(8,128)S(1)} %exponential_select_fusion.2, f32[4,128,64]{1,2,0:T(8,128)S(1)} %dynamic-slice_bitcast_fusion.9, f32[4,128,64]{1,2,0:T(8,128)S(1)} %get-tuple-element.298), kind=kLoop, calls=%fused_computation.4.clone.1 | loop fusion | flops 6275072 | bytes 8716288 | tf_op jit(solution)/shard_map/while/body/eval_jaxpr/htk,hsk,htsk->hts/dot_general | solution.py:296
  126.4 1.0 fusion.132
  129.0 1.7 exponential_select_fusion.2
  130.7 7.3 %fusion.130 = f32[4,64,64]{1,2,0:T(8,128)S(1)} fusion(f32[4,64,64,128]{3,2,1,0:T(8,128)S(1)} %exponential_select_fusion.2, f32[4,128,64]{1,2,0:T(8,128)S(1)} %dynamic-slice_bitcast_fusion.9, f32[4,128,64]{1,2,0:T(8,128)S(1)} %get-tuple-element.298), kind=kLoop, calls=%fused_computation.4.clone.1 | loop fusion | flops 6275072 | bytes 8716288 | tf_op jit(solution)/shard_map/while/body/eval_jaxpr/htk,hsk,htsk->hts/dot_general | solution.py:296
  138.4 1.0 fusion.132
  143.0 1.3 collective-permute-start
  144.7 21.7 %all-gather.2 = f32[16,4,128]{2,1,0:T(4,128)S(1)} all-gather(f32[1,4,128]{2,1,0:T(4,128)S(1)} %exponential_bitcast_fusion), channel_id=2, replica_groups=mesh['sp'=16,'tp'=2] {'sp'}, dimensions={0}, use_global_device_ids=true | all-gather | bytes 34816 | tf_op jit(solution)/shard_map/all_gather | solution.py:18
  166.4 1.7 fusion.98
  168.4 23.6 %all-gather.11.cloned.1.call-done = f32[64,128,128]{2,1,0:T(8,128)} async-done(((f32[4,128,128]{2,1,0:T(8,128)}), f32[64,128,128]{2,1,0:T(8,128)}) %all-gather.11.cloned.1.call-update) | async-done | bytes 4194320 | tf_op jit(solution)/shard_map/all_gather | solution.py:18
  193.7 1.4 fusion.96
  195.0 38.7 %all-gather.7.cloned.1.call-done = bf16[512,2048]{1,0:T(8,128)(2,1)} async-done(((bf16[512,128]{1,0:T(8,128)(2,1)}), bf16[512,2048]{1,0:T(8,128)(2,1)}) %all-gather.7.cloned.1.call-update) | async-done | bytes 2097168 | tf_op jit(solution)/shard_map/all_gather | solution.py:405
  233.8 42.3 %all-gather.9.cloned.1.call-done = bf16[512,2048]{1,0:T(8,128)(2,1)} async-done(((bf16[512,128]{1,0:T(8,128)(2,1)}), bf16[512,2048]{1,0:T(8,128)(2,1)}) %all-gather.9.cloned.1.call-update) | async-done | bytes 2097168 | tf_op jit(solution)/shard_map/all_gather | solution.py:406
  276.1 4.5 %fusion.29 = bf16[256,2048]{1,0:T(8,128)(2,1)} fusion(bf16[512,2048]{1,0:T(8,128)(2,1)} %all-gather.9.cloned.1.call-done, bf16[512,2048]{1,0:T(8,128)(2,1)} %all-gather.7.cloned.1.call-done, bf16[256,512]{1,0:T(8,128)(2,1)S(1)} %get-tuple-element.177, bf16[256,512]{1,0:T(8,128)(2,1)S(1)} %get-tuple-element.176), kind=kOutput, calls=%fused_computation.57 | convolution fusion | flops 1083703296 | bytes 5767168 | tf_op jit(solution)/shard_map/dot_general | solution.py:411
  280.6 19.6 %reduce-scatter.2.cloned.1.call-done = bf16[128,2048]{1,0:T(8,128)(2,1)} async-done(((bf16[256,2048]{1,0:T(8,128)(2,1)}), bf16[128,2048]{1,0:T(8,128)(2,1)}) %reduce-scatter.2.cloned.1.call-update) | async-done | bytes 524304 | tf_op jit(solution)/shard_map/reduce_scatter | solution.py:410
  300.3 1.2 fusion.34
  301.5 2.0 fusion.36
  (99 shorter events, 16.7 us)
Async XLA Ops:
  6.5 159.9 %copy-start = (bf16[4,128,128]{2,1,0:T(8,128)(2,1)S(1)}, bf16[4,128,128]{2,1,0:T(8,128)(2,1)}, u32[]{:S(2)}) copy-start(bf16[4,128,128]{2,1,0:T(8,128)(2,1)} %param.31) | copy-start | bytes 393220
  6.5 185.5 %all-gather.11.cloned.1.call-start = ((), (), s32[]{:S(2)}) async-start(), calls=%async_computation.4 | async-start | bytes 4456448 | tf_op jit(solution)/shard_map/all_gather | solution.py:18
  13.6 0.9 copy-start.5
  92.5 73.9 %copy-start.2 = (f32[256,512]{1,0:T(8,128)S(1)}, f32[256,512]{1,0:T(8,128)}, u32[]{:S(2)}) copy-start(f32[256,512]{1,0:T(8,128)} %get-tuple-element.180) | copy-start | bytes 1572868
  140.8 0.7 copy-start.1
  141.5 92.3 %all-gather.7.cloned.1.call-start = ((), (), s32[]{:S(2)}) async-start(), calls=%async_computation.1 | async-start | bytes 2228224 | tf_op jit(solution)/shard_map/all_gather | solution.py:405
  142.3 133.8 %all-gather.9.cloned.1.call-start = ((), (), s32[]{:S(2)}) async-start(), calls=%async_computation.2 | async-start | bytes 2228224 | tf_op jit(solution)/shard_map/all_gather | solution.py:406
  143.0 23.4 %collective-permute-start = (bf16[16,512]{1,0:T(8,128)(2,1)S(1)}, bf16[16,512]{1,0:T(8,128)(2,1)S(1)}, u32[]{:S(2)}, u32[]{:S(2)}) collective-permute-start(bf16[16,512]{1,0:T(8,128)(2,1)S(1)} %slice.75), channel_id=1, source_target_pairs={{0,2},{2,4},{4,6},{6,8},{8,10},{10,12},{12,14},{14,16},{16,18},{18... | collective-permute-start | bytes 49160 | tf_op jit(solution)/shard_map/ppermute | solution.py:32
  144.4 155.9 %reduce-scatter.2.cloned.1.call-start = ((), (), s32[]{:S(2)}) async-start(), calls=%async_computation.3 | async-start | bytes 1572864 | tf_op jit(solution)/shard_map/reduce_scatter | solution.py:410
  168.1 23.9 %copy-start.3 = (f32[4,4,64,128]{3,2,0,1:T(8,128)S(1)}, f32[4,4,64,128]{3,2,0,1:T(8,128)}, u32[]{:S(2)}) copy-start(f32[4,4,64,128]{3,2,0,1:T(8,128)} %get-tuple-element.104) | copy-start | bytes 1572868
  168.2 23.9 %copy-start.4 = (f32[4,4,64,128]{3,2,0,1:T(8,128)S(1)}, f32[4,4,64,128]{3,2,0,1:T(8,128)}, u32[]{:S(2)}) copy-start(f32[4,4,64,128]{3,2,0,1:T(8,128)} %get-tuple-element.108) | copy-start | bytes 1572868
  168.4 25.3 %copy-start.7 = (f32[512]{0:T(512)S(1)}, f32[512]{0:T(512)}, u32[]{:S(2)}) copy-start(f32[512]{0:T(512)} %param.30) | copy-start | bytes 6148
  168.4 25.3 %copy-start.8 = (f32[512]{0:T(512)S(1)}, f32[512]{0:T(512)}, u32[]{:S(2)}) copy-start(f32[512]{0:T(512)} %param.32) | copy-start | bytes 6148
  276.1 25.4 %copy-start.6 = (f32[2048]{0:T(1024)S(1)}, f32[2048]{0:T(1024)}, u32[]{:S(2)}) copy-start(f32[2048]{0:T(1024)} %param.35) | copy-start | bytes 24580
Sparse Core Ops, SparseCore 0:
  141.6 50.3 all-gather.10
  194.2 39.5 all-gather.6
  235.9 40.1 all-gather.8
  280.7 19.4 reduce-scatter.1

commit v2 on v1

--- a/solution.py
+++ b/solution.py
@@ -1,3 +1,5 @@
+import functools
+
 import jax
 import jax.numpy as jnp
 from jax import lax
@@ -6,30 +8,10 @@
 from jax.sharding import PartitionSpec as P
 
 DK = 128
-BLOCK = 64
 
 
 eps = 1e-06
 coarsest_scale_depth = lax.Precision.HIGHEST
-
-
-def prefix(part, axis, combine, identity):
-    place = lax.axis_index(axis)
-    gathered = jax.tree.map(lambda a: lax.all_gather(a, axis), part)
-    state = jax.tree.map(lambda a, e: jnp.zeros_like(a) + jnp.asarray(e, a.dtype), part, identity)
-
-    def one(turn, state):
-        return combine(
-            state, jax.tree.map(lambda a: lax.dynamic_index_in_dim(a, turn, 0, False), gathered)
-        )
-
-    return lax.fori_loop(0, place, one, state)
-
-
-def shifted(value, axis, steps):
-    count = lax.axis_size(axis)
-    initial, last = (max(0, -steps), min(count, count - steps))
-    return lax.ppermute(value, axis, [(source, source + steps) for source in range(initial, last)])
 
 
 PIECES = 2
@@ -236,8 +218,6 @@
 
 
 def project(tokens, gain, shard):
-    import functools
-
     n = lax.axis_size("sp")
     n_tp = lax.axis_size("tp")
     positions, features = tokens.shape
@@ -272,47 +252,398 @@
     )(tokens, gain[None, :], shard)
 
 
-def chain_merge(earlier, later):
-    return (earlier[0] * later[0], later[0][..., None] * earlier[1] + later[1])
-
-
-def local_blocks(qs, keys, values, logs):
-    causal = jnp.arange(BLOCK)[:, None] >= jnp.arange(BLOCK)[None, :]
-    heads_dev = qs.shape[1]
-
-    def advance(carry, member):
-        carried_memory_matrix, start = carry
-        probe_segment, key_piece, input_piece, gc = member
-        prefix_sum_vector = jnp.cumsum(gc, axis=1)
-        last_index = prefix_sum_vector[:, -1]
-        cross_segment_contribution = jnp.einsum(
-            "abz,azy->aby",
-            probe_segment * jnp.exp(prefix_sum_vector),
-            carried_memory_matrix,
-            precision=coarsest_scale_depth,
-        )
-        diff = prefix_sum_vector[:, :, None, :] - prefix_sum_vector[:, None, :, :]
-        weight = jnp.where(causal[None, :, :, None], jnp.exp(jnp.minimum(diff, 0.0)), 0.0)
-        scores = jnp.einsum(
-            "htk,hsk,htsk->hts", probe_segment, key_piece, weight, precision=coarsest_scale_depth
-        )
-        final_result = cross_segment_contribution + jnp.einsum(
-            "hts,hsv->htv", scores, input_piece, precision=coarsest_scale_depth
-        )
-        carried_memory_matrix = jnp.exp(last_index)[..., None] * carried_memory_matrix + jnp.einsum(
-            "njp,njq->npq",
-            key_piece * jnp.exp(last_index[:, None, :] - prefix_sum_vector),
-            input_piece,
-            precision=coarsest_scale_depth,
-        )
-        pool_reach = probe_segment * jnp.exp(start[:, None, :] + prefix_sum_vector)
-        return ((carried_memory_matrix, start + last_index), (final_result, pool_reach))
-
-    begin = (jnp.zeros((heads_dev, DK, DK), jnp.float32), jnp.zeros((heads_dev, DK), jnp.float32))
-    (carried_memory_matrix, total), (final_result, pool_reach) = lax.scan(
-        advance, begin, (qs, keys, values, logs)
+def mix_kernel(
+    n,
+    n_tp,
+    proj_ref,
+    keep_ref,
+    extra_ref,
+    sgain_ref,
+    mix_ref,
+    pgain_ref,
+    w_ref,
+    post_ref,
+    out_ref,
+    weights,
+    local,
+    reach,
+    both,
+    state,
+    before,
+    gone_state,
+    gone_decay,
+    come_state,
+    come_decay,
+    tail,
+    tail_in,
+    mine,
+    gone_out,
+    come_out,
+    ring_send,
+    ring_recv,
+    core_send,
+    core_recv,
+    scan_send,
+    scan_recv,
+    tail_sem,
+    own_sem,
+    out_send,
+    out_recv,
+):
+    f32, bf16 = jnp.float32, jnp.bfloat16
+    chips = n // 2
+    steps = chips // 2
+    rounds = (n - 1).bit_length()
+    me = lax.axis_index("sp")
+    tp = lax.axis_index("tp")
+    core = me % 2
+    place = ring_place(me // 2, chips)
+
+    def chip_at(offset):
+        return ring_chip((place + offset + chips) % chips, chips)
+
+    following = 2 * chip_at(1) + core
+    preceding = 2 * chip_at(-1) + core
+    partner = 2 * (me // 2) + 1 - core
+    piece = w_ref.shape[0] // PIECES
+
+    barrier = pltpu.get_barrier_semaphore()
+    for peer in (following, preceding, partner):
+        pl.semaphore_signal(barrier, inc=1, device_id={"sp": peer})
+    for r in range(rounds):
+        pl.semaphore_signal(barrier, inc=1, device_id={"sp": (me + 2**r) % n})
+        pl.semaphore_signal(barrier, inc=1, device_id={"sp": (me - 2**r + n) % n})
+    for turn in range(1, n_tp):
+        pl.semaphore_signal(barrier, inc=1, device_id={"tp": (tp + turn) % n_tp})
+    pl.semaphore_wait(barrier, 3 + 2 * rounds + n_tp - 1)
+
+    sends = []
+
+    def spot(chip, which, q):
+        return weights.at[2 * chip + which, pl.ds(q * piece, piece)]
+
+    def to_core(offset, q, source):
+        slot = offset + steps - 1
+        copy = pltpu.make_async_remote_copy(
+            src_ref=source,
+            dst_ref=spot(chip_at(offset), core, q),
+            send_sem=core_send.at[slot, q],
+            recv_sem=core_recv.at[slot, q],
+            device_id={"sp": partner},
+        )
+        copy.start()
+        sends.append(copy)
+
+    def from_core(offset, q):
+        slot = offset + steps - 1
+        dst = spot(chip_at(offset), 1 - core, q)
+        pltpu.make_async_remote_copy(
+            src_ref=dst,
+            dst_ref=dst,
+            send_sem=core_send.at[slot, q],
+            recv_sem=core_recv.at[slot, q],
+            device_id={"sp": partner},
+        ).wait_recv()
+
+    def pieces_of(direction, step):
+        if step < steps - 1:
+            return range(PIECES)
+        half = PIECES // 2
+        return range(half) if direction == 0 else range(half, PIECES)
+
+    def ring_copy(direction, step, q, source, offset):
+        dst = spot(chip_at(offset), core, q)
+        return pltpu.make_async_remote_copy(
+            src_ref=dst if source is None else source,
+            dst_ref=dst,
+            send_sem=ring_send.at[direction, step, q],
+            recv_sem=ring_recv.at[direction, step, q],
+            device_id={"sp": following if direction == 0 else preceding},
+        )
+
+    def ring_step(step):
+        for q in range(PIECES):
+            for direction in range(2):
+                if q not in pieces_of(direction, step):
+                    continue
+                offset = -(step + 1) if direction == 0 else step + 1
+                ring_copy(direction, step, q, None, offset).wait_recv()
+                if step + 1 < steps and q in pieces_of(direction, step + 1):
+                    copy = ring_copy(direction, step + 1, q, None, offset)
+                    copy.start()
+                    sends.append(copy)
+                last = offset if abs(offset) < steps else steps
+                to_core(last, q, spot(chip_at(last), core, q))
+
+    pending = list(range(steps))
+
+    def advance_ring():
+        if pending:
+            ring_step(pending.pop(0))
+
+    positions = proj_ref.shape[0]
+    head_cols = proj_ref.shape[1] // 6
+    heads = head_cols // DK
+    reach_back = tail.shape[0]
+
+    tail[...] = proj_ref[positions - reach_back :, 4 * head_cols : 5 * head_cols]
+    for q in range(PIECES):
+        own_piece = w_ref.at[pl.ds(q * piece, piece)]
+        for direction in range(2):
+            if q in pieces_of(direction, 0):
+                copy = ring_copy(direction, 0, q, own_piece, 0)
+                copy.start()
+                sends.append(copy)
+        to_core(0, q, own_piece)
+    own = pltpu.make_async_copy(w_ref, weights.at[me], own_sem)
+    own.start()
+    tail_copy = pltpu.make_async_remote_copy(
+        src_ref=tail,
+        dst_ref=tail_in,
+        send_sem=tail_sem.at[0],
+        recv_sem=tail_sem.at[1],
+        device_id={"sp": (me + 1) % n},
     )
-    return (carried_memory_matrix, total, final_result, pool_reach)
+    tail_copy.start()
+
+    row = lax.broadcasted_iota(jnp.int32, (positions, positions), 0)
+    col = lax.broadcasted_iota(jnp.int32, (positions, positions), 1)
+    lower = jnp.where(row >= col, 1.0, 0.0).astype(f32)
+    line = lax.broadcasted_iota(jnp.int32, (positions, DK), 0)
+    units = positions // 8
+    sub = lax.broadcasted_iota(jnp.int32, (units, 8, DK), 1)
+    over_last = (((1,), (1,)), ((), ()))
+
+    decay_now = []
+    for h in range(heads):
+        at = slice(h * DK, (h + 1) * DK)
+        part = lambda i: proj_ref[:, i * head_cols + h * DK : i * head_cols + (h + 1) * DK]
+        q = part(0).astype(f32) * DK ** (-0.5)
+        kg = keep_ref[:, at] * jax.nn.sigmoid(-part(1).astype(f32))
+        v = part(2)
+        logs = jnp.log1p(-kg) + extra_ref[:, h : h + 1]
+        c = jnp.dot(
+            lower, logs, precision=coarsest_scale_depth, preferred_element_type=f32
+        )
+        last = c[positions - 1 :, :]
+        state[h] = lax.dot_general(
+            v,
+            (kg * jnp.exp(last - c)).astype(bf16),
+            (((0,), (0,)), ((), ())),
+            preferred_element_type=f32,
+        )
+        gone_decay[0, h : h + 1, :] = jnp.exp(last)
+        reach[:, at] = (q * jnp.exp(c)).astype(bf16)
+        scores = jnp.zeros((positions, positions), f32)
+        span = 8
+        while span < positions:
+            pair = 2 * span
+            c3 = c.reshape(positions // pair, pair, DK)
+            middle = jnp.broadcast_to(c3[:, span - 1 : span, :], c3.shape).reshape(c.shape)
+            fade = jnp.exp(-jnp.abs(c - middle))
+            later = (line // span) % 2 == 1
+            probe = jnp.where(later, q * fade, 0.0).astype(bf16)
+            keyed = jnp.where(later, 0.0, kg * fade).astype(bf16)
+            found = lax.dot_general(probe, keyed, over_last, preferred_element_type=f32)
+            scores = scores + jnp.where(row // pair == col // pair, found, 0.0)
+            span = pair
+        result = jnp.dot(scores.astype(bf16), v, preferred_element_type=f32)
+        c3 = c.reshape(units, 8, DK)
+        q3 = q.reshape(units, 8, DK)
+        k3 = kg.reshape(units, 8, DK)
+        v3 = v.astype(f32).reshape(units, 8, DK)
+        near = result.reshape(units, 8, DK)
+        for s in range(8):
+            weight = jnp.exp(jnp.minimum(c3 - c3[:, s : s + 1, :], 0.0))
+            score = jnp.sum(q3 * k3[:, s : s + 1, :] * weight, axis=2, keepdims=True)
+            near = near + jnp.where(sub >= s, score * v3[:, s : s + 1, :], 0.0)
+        local[:, at] = near.reshape(positions, DK)
+        if h % 2 == 1:
+            advance_ring()
+
+    def scan_copies(r):
+        target = {"sp": (me + 2**r) % n}
+        return [
+            pltpu.make_async_remote_copy(
+                src_ref=gone.at[r],
+                dst_ref=come.at[r],
+                send_sem=scan_send.at[r, i],
+                recv_sem=scan_recv.at[r, i],
+                device_id=target,
+            )
+            for i, (gone, come) in enumerate(
+                [(gone_state, come_state), (gone_decay, come_decay)]
+            )
+        ]
+
+    before[...] = jnp.zeros_like(before)
+    decay_w = [gone_decay[0, h : h + 1, :] for h in range(heads)]
+    decay_e = [jnp.ones((1, DK), f32) for h in range(heads)]
+
+    def pool(h):
+        at = slice(h * DK, (h + 1) * DK)
+        x = proj_ref[:, 4 * head_cols + h * DK : 4 * head_cols + (h + 1) * DK].astype(f32)
+        prior = jnp.where(me > 0, tail_in[:, at].astype(f32), 0.0)
+        level = (tp * heads + h) % 4
+        total = jnp.concatenate([prior, x], axis=0)
+        chosen = jnp.zeros((positions, DK), f32)
+        for k in range(4):
+            total = total + pltpu.roll(total, 2**k, 0)
+            chosen = jnp.where(level == k, total[reach_back:, :], chosen)
+        window = 2
+        for k in range(1, 4):
+            window = jnp.where(level == k, 2 ** (1 + k), window)
+        count = jnp.minimum(me * positions + line + 1, window).astype(f32)
+        mixed = (chosen / count - x).astype(bf16)
+        mapped = jnp.dot(mixed, mix_ref[h], preferred_element_type=f32)
+        gate = proj_ref[:, 5 * head_cols + h * DK : 5 * head_cols + (h + 1) * DK].astype(f32)
+        both[:, head_cols + h * DK : head_cols + (h + 1) * DK] = (
+            mapped * pgain_ref[:, at] * (gate * jax.nn.sigmoid(gate))
+        ).astype(bf16)
+
+    pools = list(range(heads))
+    for r in range(rounds):
+        gone_state[r] = state[...].astype(bf16)
+        if r > 0:
+            for h in range(heads):
+                gone_decay[r, h : h + 1, :] = decay_w[h]
+        for copy in scan_copies(r):
+            copy.start()
+            sends.append(copy)
+        if r == 0:
+            tail_copy.wait_recv()
+        if pools:
+            pool(pools.pop(0))
+        advance_ring()
+        for copy in scan_copies(r):
+            copy.wait_recv()
+        valid = me >= 2**r
+        for h in range(heads):
+            came = jnp.where(valid, come_state[r, h].astype(f32), 0.0)
+            came_decay = jnp.where(valid, come_decay[r, h : h + 1, :], 1.0)
+            before[h] = before[h] + decay_e[h] * came
+            decay_e[h] = decay_e[h] * came_decay
+            if r + 1 < rounds:
+                state[h] = state[h] + decay_w[h] * came
+                decay_w[h] = decay_w[h] * came_decay
+    for h in pools:
+        pool(h)
+    while pending:
+        advance_ring()
+
+    for h in range(heads):
+        at = slice(h * DK, (h + 1) * DK)
+        rec = local[:, at] + lax.dot_general(
+            reach[:, at], before[h].astype(bf16), over_last, preferred_element_type=f32
+        )
+        normed = rec * lax.rsqrt(jnp.mean(rec * rec, axis=1, keepdims=True) + eps)
+        gate = proj_ref[:, 3 * head_cols + h * DK : 3 * head_cols + (h + 1) * DK].astype(f32)
+        both[:, at] = (normed * sgain_ref[:, at] * (gate * jax.nn.sigmoid(gate))).astype(bf16)
+
+    own.wait()
+    for offset in range(-(steps - 1), steps + 1):
+        for q in range(PIECES):
+            from_core(offset, q)
+
+    owned = positions // n_tp
+    width = w_ref.shape[1]
+    quarter = n // 4
+
+    def share(rows, group):
+        left = both[rows, :]
+        for slot in range(group * quarter, (group + 1) * quarter, 2):
+            right = jnp.concatenate([weights[slot], weights[slot + 1]], axis=1)
+            yield slot, jnp.dot(left, right, preferred_element_type=f32).astype(bf16)
+
+    def out_copy(turn, group):
+        cols = pl.ds(group * quarter * width, quarter * width)
+        return pltpu.make_async_remote_copy(
+            src_ref=gone_out.at[turn - 1, :, cols],
+            dst_ref=come_out.at[turn - 1, :, cols],
+            send_sem=out_send.at[turn - 1, group],
+            recv_sem=out_recv.at[turn - 1, group],
+            device_id={"tp": (tp + turn) % n_tp},
+        )
+
+    for turn in range(1, n_tp):
+        target = (tp + turn) % n_tp
+        rows = pl.ds(pl.multiple_of(target * owned, owned), owned)
+        for group in range(4):
+            for slot, value in share(rows, group):
+                gone_out[turn - 1, :, slot * width : (slot + 2) * width] = value
+            copy = out_copy(turn, group)
+            copy.start()
+            sends.append(copy)
+    rows = pl.ds(pl.multiple_of(tp * owned, owned), owned)
+    for group in range(4):
+        for slot, value in share(rows, group):
+            mine[:, slot * width : (slot + 2) * width] = value.astype(f32)
+    for turn in range(1, n_tp):
+        for group in range(4):
+            out_copy(turn, group).wait_recv()
+        mine[...] += come_out[turn - 1].astype(f32)
+    summed = mine[...]
+    out_ref[...] = (
+        summed
+        * lax.rsqrt(jnp.mean(summed * summed, axis=1, keepdims=True) + eps)
+        * post_ref[...]
+    ).astype(bf16)
+    tail_copy.wait_send()
+    for copy in sends:
+        copy.wait_send()
+
+
+def mix(proj, keep, extra, sgain, pool_mix, pgain, shard, post):
+    n = lax.axis_size("sp")
+    n_tp = lax.axis_size("tp")
+    positions, heads = extra.shape
+    head_cols = heads * DK
+    depth, width = shard.shape
+    steps = n // 4
+    rounds = (n - 1).bit_length()
+    owned = positions // n_tp
+    model = n * width
+    padded = -(-heads // 8) * 8
+    f32, bf16, dma = jnp.float32, jnp.bfloat16, pltpu.SemaphoreType.DMA
+    return pl.pallas_call(
+        functools.partial(mix_kernel, n, n_tp),
+        out_shape=jax.ShapeDtypeStruct((owned, model), bf16),
+        in_specs=[pl.BlockSpec(memory_space=pltpu.VMEM)] * 8,
+        out_specs=pl.BlockSpec(memory_space=pltpu.VMEM),
+        scratch_shapes=[
+            pltpu.VMEM((n, depth, width), bf16),
+            pltpu.VMEM((positions, head_cols), f32),
+            pltpu.VMEM((positions, head_cols), bf16),
+            pltpu.VMEM((positions, 2 * head_cols), bf16),
+            pltpu.VMEM((heads, DK, DK), f32),
+            pltpu.VMEM((heads, DK, DK), f32),
+            pltpu.VMEM((rounds, heads, DK, DK), bf16),
+            pltpu.VMEM((rounds, padded, DK), f32),
+            pltpu.VMEM((rounds, heads, DK, DK), bf16),
+            pltpu.VMEM((rounds, padded, DK), f32),
+            pltpu.VMEM((16, head_cols), bf16),
+            pltpu.VMEM((16, head_cols), bf16),
+            pltpu.VMEM((owned, model), f32),
+            pltpu.VMEM((n_tp, owned, model), bf16),
+            pltpu.VMEM((n_tp, owned, model), bf16),
+            dma((2, steps, PIECES)),
+            dma((2, steps, PIECES)),
+            dma((2 * steps, PIECES)),
+            dma((2 * steps, PIECES)),
+            dma((rounds, 2)),
+            dma((rounds, 2)),
+            dma((2,)),
+            dma,
+            dma((n_tp, 4)),
+            dma((n_tp, 4)),
+        ],
+        compiler_params=pltpu.CompilerParams(
+            collective_id=1, has_side_effects=True, vmem_limit_bytes=56 * 1024 * 1024
+        ),
+        cost_estimate=pl.CostEstimate(
+            flops=2 * positions * depth * model, bytes_accessed=4 * depth * width, transcendentals=0
+        ),
+    )(proj, keep, extra, sgain, pool_mix, pgain, shard, post)
 
 
 def per_device(
@@ -336,89 +667,17 @@
     shard = jnp.concatenate(
         [w_query, w_forget, w_input, w_rgate, w_pool_in, w_pgate], axis=1
     )
-    head_cols = w_query.shape[1]
-    positions = tokens_in.shape[0]
     proj = project(tokens_in, norm_gain, shard)
-    query = proj[:, 0:head_cols]
-    forget = proj[:, head_cols : 2 * head_cols]
-    inputs = proj[:, 2 * head_cols : 3 * head_cols]
-    rgate = proj[:, 3 * head_cols : 4 * head_cols]
-    pool_in = proj[:, 4 * head_cols : 5 * head_cols]
-    pgate = proj[:, 5 * head_cols : 6 * head_cols]
-    heads_dev = head_cols // DK
-    blocks = positions // BLOCK
-
-    def to_blocks(array):
-        return array.reshape(blocks, BLOCK, heads_dev, DK).transpose(0, 2, 1, 3)
-
-    forget32 = forget.astype(jnp.float32)
-    key_gate = -jnp.expm1(-floor_rate)[None, :] * jax.nn.sigmoid(-forget32)
-    log_forget = jnp.log1p(-key_gate) + jnp.repeat(extra_logdecay, DK, axis=1)
-    qs = query.astype(jnp.float32) * DK ** (-0.5)
-    carried_memory_matrix, total, final_result, pool_reach = local_blocks(
-        to_blocks(qs),
-        to_blocks(key_gate),
-        to_blocks(inputs.astype(jnp.float32)),
-        to_blocks(log_forget),
+    return mix(
+        proj,
+        -jnp.expm1(-floor_rate)[None, :],
+        extra_logdecay,
+        state_gain[None, :],
+        pool_mix,
+        pool_gain[None, :],
+        jnp.concatenate([out_rec, out_pool], axis=0),
+        post_gain[None, :],
     )
-    decays = jnp.exp(total)
-    tail_rows = pool_in[positions - 16 :]
-    carried = prefix(
-        (decays, carried_memory_matrix),
-        "sp",
-        chain_merge,
-        (jnp.ones_like(decays), jnp.zeros_like(carried_memory_matrix)),
-    )
-    incoming_state = carried[1]
-    previous = shifted(tail_rows, "sp", 1).astype(jnp.float32)
-    recurrent_output = final_result + jnp.einsum(
-        "izaf,zfu->izau", pool_reach, incoming_state, precision=coarsest_scale_depth
-    )
-    grouped = recurrent_output.transpose(0, 2, 1, 3).reshape(positions, heads_dev, DK)
-    normed = grouped * lax.rsqrt(jnp.mean(grouped * grouped, axis=2, keepdims=True) + eps)
-    y_rec = (
-        normed.reshape(positions, head_cols)
-        * state_gain[None, :]
-        * jax.nn.silu(rgate.astype(jnp.float32))
-    ).astype(jnp.bfloat16)
-    group = lax.axis_index("tp") * heads_dev + jnp.arange(head_cols) // DK
-    window = jnp.power(2, 1 + group % 4).astype(jnp.int32)
-    pool32 = pool_in.astype(jnp.float32)
-    extended = jnp.concatenate([previous, pool32], axis=0)
-    summed_rows = jnp.zeros((positions, head_cols), jnp.float32)
-    for offset in range(16):
-        rows_back = extended[16 - offset : 16 - offset + positions]
-        summed_rows = summed_rows + jnp.where((offset < window)[None, :], rows_back, 0.0)
-    place = lax.axis_index("sp") * positions + jnp.arange(positions)
-    count = jnp.minimum(place[:, None] + 1, window[None, :]).astype(jnp.float32)
-    mixed = (summed_rows / count - pool32).astype(jnp.bfloat16)
-    mapped = jnp.einsum(
-        "tgc,gcd->tgd",
-        mixed.reshape(positions, heads_dev, DK),
-        pool_mix,
-        preferred_element_type=jnp.float32,
-    ).reshape(positions, head_cols)
-    y_pool = (mapped * pool_gain[None, :] * jax.nn.silu(pgate.astype(jnp.float32))).astype(
-        jnp.bfloat16
-    )
-    out_parts = (
-        lax.all_gather(out_rec, "sp", axis=1, tiled=True),
-        lax.all_gather(out_pool, "sp", axis=1, tiled=True),
-    )
-    both = jnp.concatenate([y_rec, y_pool], axis=1)
-    weight_cat = jnp.concatenate(out_parts, axis=0)
-    summed = lax.psum_scatter(
-        jnp.dot(both, weight_cat, preferred_element_type=jnp.float32).astype(jnp.bfloat16),
-        "tp",
-        scatter_dimension=0,
-        tiled=True,
-    ).astype(jnp.float32)
-    final = (
-        summed
-        * lax.rsqrt(jnp.mean(summed * summed, axis=1, keepdims=True) + eps)
-        * post_gain[None, :]
-    )
-    return final.astype(jnp.bfloat16)
 
 
 def solution(mesh):

time: 311 us -> 139 us (0.45)
  waiting for transfers between devices: 125 us -> 0 us
  Pallas kernels: 73.3 us -> 128 us
  other arithmetic: 48.3 us -> 1.32 us
  blocking collectives: 21.7 us -> 0 us
  matrix products: 15.2 us -> 0 us
  between operations: 13.4 us -> 0.07 us
    all_gather x3 -> x0, waiting for transfers between devices: 105 us -> none  [the longest x1 42.3 us: per_device(): lax.all_gather(out_pool, 'sp', axis=1, tiled=True)]
    pallas_call x0 -> x1, Pallas kernels: none -> 54.3 us  [mix(): pl.pallas_call(functools.partial(mix_kernel, n, n_tp), out_shape=jax.Shap...]
    dot_general x4 -> x0, other arithmetic: 29.3 us -> none  [advance(): jnp.einsum('htk,hsk,htsk->hts', probe_segment, key_piece, weight, precisi...]
    all_gather x1 -> x0, blocking collectives: 21.7 us -> none  [prefix(): gathered = jax.tree.map(lambda a: lax.all_gather(a, axis), part)]
    reduce_scatter x1 -> x0, waiting for transfers between devices: 19.6 us -> none  [per_device(): lax.psum_scatter(jnp.dot(both, weight_cat, preferred_element_type=jnp.flo...]
    dot_general x15 -> x0, matrix products: 15.2 us -> none  [the longest x1 4.49 us: per_device(): jnp.dot(both, weight_cat, preferred_element_type=jnp.float32)]
    select_n x5 -> x0, other arithmetic: 6.77 us -> none  [the longest x4 6.75 us: advance(): jnp.where(causal[None, :, :, None], jnp.exp(jnp.minimum(diff, 0.0)), 0.0)]
    convert_element_type x3 -> x0, other arithmetic: 3.4 us -> none  [the longest x1 2.02 us: per_device(): return final.astype(jnp.bfloat16)]
  transfers between devices with their start and end apart: 5 -> 0, of which waited for: 4 -> 0; matrix products, arithmetic and copies ran while one was open for 2% -> 0% of each run, Pallas kernels for 0% -> 0%
where the time goes in v2:
time: 139 us; the launch traced here: 138 us
  Pallas kernels  128 us (92%)
  local copies, waits for them, and re-layouts  9.08 us (7%)
    pallas_call x1, Pallas kernels, project(): pl.pallas_call(functools.partial(project_kernel, n, n_tp), out_shape=jax....  73.3 us
    pallas_call x1, Pallas kernels, mix(): pl.pallas_call(functools.partial(mix_kernel, n, n_tp), out_shape=jax.Shap...  54.3 us
    unnamed x17, local copies, waits for them, and re-layouts  8.17 us

profile of v2, /device:TPU:0, one launch (start us, length us, event | category | flops | bytes accessed | tf_op | source)
XLA Modules:
  0.0 138.1 jit_solution(2559674065151798536)
XLA Ops:
  0.0 0.9 constant_dynamic-update-slice_fusion.5
  0.9 0.9 constant_dynamic-update-slice_fusion.4
  1.8 0.9 constant_dynamic-update-slice_fusion.3
  2.8 0.9 constant_dynamic-update-slice_fusion.2
  3.7 0.9 constant_dynamic-update-slice_fusion.1
  4.6 0.9 constant_dynamic-update-slice_fusion.w_ref
  5.5 0.0 copy-start.2
  5.5 0.9 copy-done.2
  6.4 0.0 copy-start
  6.4 0.0 copy-start.1
  6.4 0.0 copy-start.3
  6.4 0.0 copy-start.4
  6.4 73.3 %shard_map.154.proj_ref = bf16[256,3072]{1,0:T(8,128)(2,1)} custom-call(bf16[256,1024]{1,0:T(8,128)(2,1)} %tok_ref.1, f32[1,2048]{1,0:T(1,128)} %bitcast.6, bf16[128,3072]{1,0:T(8,128)(2,1)} %copy-done.2), custom_call_target="tpu_custom_call" | custom-call | flops 3221225472 | bytes 1572864 | tf_op jit(solution)/shard_map/pallas_call | solution.py:228
  79.8 0.0 copy-done
  79.8 0.0 copy-done.1
  79.8 0.7 pad_maximum_fusion.w_ref
  80.5 0.0 copy-done.3
  80.5 0.8 copy.17.extra_ref
  81.3 0.0 copy-done.4
  81.3 0.6 exponential-minus-one_negate_fusion
  81.9 54.3 %shard_map.155 = bf16[128,2048]{1,0:T(8,128)(2,1)} custom-call(bf16[256,3072]{1,0:T(8,128)(2,1)} %shard_map.154.proj_ref, f32[1,512]{1,0:T(1,128)} %bitcast.5, f32[256,4]{1,0:T(8,128)} %copy.17.extra_ref, f32[1,512]{1,0:T(1,128)} %bitcast.8, bf16[4,128,128]{2,1,0:T(8,128)(2,1)} %mix_ref.1, f32[1,512]{1,0:T(1,128)} %bitcast.9, ...), custom_call_target="tpu_custom_call" | custom-call | flops 1073741824 | bytes 524288 | tf_op jit(solution)/shard_map/pallas_call | solution.py:608
  136.2 1.9 %copy.24 = bf16[128,2048]{1,0:T(8,128)(2,1)} copy(bf16[128,2048]{1,0:T(8,128)(2,1)} %shard_map.155) | data formatting | bytes 1048576
Async XLA Ops:
  5.5 0.9 copy-start.2
  6.4 73.4 %copy-start = (bf16[512,128]{1,0:T(8,128)(2,1)S(1)}, bf16[512,128]{1,0:T(8,128)(2,1)}, u32[]{:S(2)}) copy-start(bf16[512,128]{1,0:T(8,128)(2,1)} %param.30) | copy-start | bytes 393220
  6.4 73.4 %copy-start.1 = (bf16[512,128]{1,0:T(8,128)(2,1)S(1)}, bf16[512,128]{1,0:T(8,128)(2,1)}, u32[]{:S(2)}) copy-start(bf16[512,128]{1,0:T(8,128)(2,1)} %param.29) | copy-start | bytes 393220
  6.4 74.1 %copy-start.3 = (f32[256,4]{0,1:T(4,128)S(1)}, f32[256,4]{0,1:T(4,128)}, u32[]{:S(2)}) copy-start(f32[256,4]{0,1:T(4,128)} %param.25) | copy-start | bytes 12292
  6.4 74.9 %copy-start.4 = (f32[512]{0:T(512)S(1)}, f32[512]{0:T(512)}, u32[]{:S(2)}) copy-start(f32[512]{0:T(512)} %param.24) | copy-start | bytes 6148
